TPU v7x, 32 devices: a whole 2x2x4 slice. The times are simulated.
32 devices in a mesh: kv: 8 (over z, y), tp: 4 (over x, core).
Axes of the slice: x: 2, y: 2, z: 4, core: 2. Of those that a mesh axis runs over, the one named last changes fastest.
Arguments:
- tokens: bfloat16 [128, 4096], P(None, 'kv'), may hold values from -152 to 152, as said below
- norm_gain: float32 [4096], P('kv'), may hold values from 0.1 to 1.9
- w_query: bfloat16 [4096, 2048], P('kv', 'tp'), may hold values from -0.09375 to 0.09375
- w_key: bfloat16 [4096, 2048], P('kv', 'tp'), may hold values from -0.375 to 0.375
- w_value: bfloat16 [4096, 2048], P('kv', 'tp'), may hold values from -0.09375 to 0.09375
- lambdas: float32 [16], P('tp'), may hold values from 0.3 to 0.8
- head_gain: float32 [128], replicated, may hold values from 0.1 to 1.9
- w_out: bfloat16 [2048, 4096], P('tp', 'kv'), may hold values from -0.125 to 0.125
- cache_keys: bfloat16 [8, 4096, 16, 128], P(None, 'kv', 'tp'), may hold values from -370 to 370
- cache_values: bfloat16 [8, 4096, 16, 128], P(None, 'kv', 'tp'), may hold values from -6 to 6
- lengths: int32 [8], replicated, may hold values from 2560 to 4074
- accepted: int32 [8], replicated, may hold values from 0 to 6
- parents: int32 [8, 16], replicated, may hold values from -1 to 14, as said below
Outputs:
- layer_out: bfloat16 [128, 4096], P('tp', 'kv')
- keys_out: bfloat16 [8, 4096, 16, 128], P(None, 'kv', 'tp')
- values_out: bfloat16 [8, 4096, 16, 128], P(None, 'kv', 'tp')
Inputs may be any that keep to these rules, and one draw needn't show every extreme that they name: `tokens`: columns of features have scales that differ; rows too. The proposals of the last step that were kept already stand right after the first lengths positions; the next 16 positions receive this step's proposals. `parents`: proposal 0 of every sequence has parent -1; every other proposal's parent is an earlier proposal of the same sequence, and the last proposal's parent is the one right before it.
All inputs are finite; a program needn't handle non-finite values.
Results may differ from a plain program's by a relative error of at most 0.015.
The roundings to bfloat16 on the way count: a program that leaves them out, or rounds other values in their place, can miss the bound.
Values may be sent and summed in bfloat16 or wider, within the bound.
A program may use at most 64 MiB of HBM per device.

v0:
```python
import jax
import jax.numpy as jnp
from jax import lax
from jax.sharding import PartitionSpec as P

D = 4096
HEAD = 64
KDIM = 128
PROP = 16
eps_row = 1e-06
eps_head = 1e-05
masked = -1e30


def ancestry(parents):
    members = parents.shape[0]
    indices = jnp.arange(members, dtype=jnp.int32)
    reachable = (parents[:, None] == indices[None, :]).astype(jnp.float32) + jnp.eye(
        members, dtype=jnp.float32
    )
    for repeat in range(max(1, (members - 1).bit_length())):
        reachable = jnp.minimum(jnp.dot(reachable, reachable, precision=lax.Precision.HIGHEST), 1.0)
    return reachable


def combine(earlier, latter):
    maxima_a, totals_a, summed_a = earlier
    maxima_b, totals_b, summed_b = latter
    highest = jnp.maximum(maxima_a, maxima_b)
    factor_a = jnp.exp(maxima_a - highest)
    factor_b = jnp.exp(maxima_b - highest)
    return (
        highest,
        totals_a * factor_a + totals_b * factor_b,
        summed_a * factor_a[..., None] + summed_b * factor_b[..., None],
    )


def softmax_block(scores, allowed, values):
    scores = jnp.where(allowed, scores, masked)
    maxima = jnp.max(scores, axis=-1)
    weights = jnp.where(allowed, jnp.exp(scores - maxima[..., None]), 0.0)
    totals = jnp.sum(weights, axis=-1)
    summed = jnp.einsum(
        "bjhmp,bphd->bjhmd",
        weights.astype(jnp.bfloat16),
        values,
        preferred_element_type=jnp.float32,
    )
    return (maxima, totals, summed)


def finish(merged, lambdas, head_gain):
    maxima, totals, summed = merged
    attended = summed / totals[..., None]
    blended = attended[..., 0, :] - lambdas[:, None] * attended[..., 1, :]
    inverse_rms = lax.rsqrt(jnp.mean(blended * blended, axis=-1, keepdims=True) + eps_head)
    return (blended * inverse_rms * head_gain).astype(jnp.bfloat16)


def leading(array, token_count):
    return array.reshape((1, token_count) + array.shape[2:])


def body(
    tokens,
    norm_gain,
    w_query,
    w_key,
    w_value,
    lambdas,
    head_gain,
    w_out,
    cache_keys,
    cache_values,
    lengths,
    accepted,
    parents,
):
    token_count = tokens.shape[0]
    sequences = token_count // PROP
    local_heads = w_query.shape[1] // KDIM
    widened = tokens.astype(jnp.float32)
    squares_local = jnp.sum(widened * widened, axis=1, keepdims=True)
    scaled = (widened * norm_gain[None, :]).astype(jnp.bfloat16)
    part_query = jnp.dot(scaled, w_query, preferred_element_type=jnp.float32)
    part_key = jnp.dot(scaled, w_key, preferred_element_type=jnp.float32)
    part_value = jnp.dot(scaled, w_value, preferred_element_type=jnp.float32)
    sum_query, sum_key, sum_value, squares = lax.psum(
        (part_query, part_key, part_value, squares_local), "kv"
    )
    row_scale = lax.rsqrt(squares / D + eps_row)
    queries = (row_scale * sum_query).astype(jnp.bfloat16)
    new_keys = (row_scale * sum_key).astype(jnp.bfloat16)
    new_values = (row_scale * sum_value).astype(jnp.bfloat16)
    query_pairs = queries.reshape(sequences, PROP, local_heads, 2, HEAD)
    key_pairs = new_keys.reshape(sequences, PROP, local_heads, 2, HEAD)
    keys_fresh = new_keys.reshape(sequences, PROP, local_heads, KDIM)
    values_fresh = new_values.reshape(sequences, PROP, local_heads, KDIM)
    cache_positions = cache_keys.shape[1]
    positions = lax.axis_index("kv") * cache_positions + jnp.arange(
        cache_positions, dtype=jnp.int32
    )
    limits = lengths + accepted
    usable = (positions[None, :] < limits[:, None])[:, None, None, None, :]
    score_scale = HEAD ** (-0.5)
    stored_pairs = cache_keys.reshape(sequences, cache_positions, local_heads, 2, HEAD)
    scores = (
        jnp.einsum(
            "bjhmd,bphmd->bjhmp", query_pairs, stored_pairs, preferred_element_type=jnp.float32
        )
        * score_scale
    )
    cache_part = softmax_block(scores, usable, cache_values)
    reachable = jax.vmap(ancestry)(parents) > 0.5
    tree_scores = (
        jnp.einsum("bjhmd,bihmd->bjhmi", query_pairs, key_pairs, preferred_element_type=jnp.float32)
        * score_scale
    )
    tree_part = softmax_block(tree_scores, reachable[:, :, None, None, :], values_fresh)
    own_rows = token_count // lax.axis_size("kv")
    first_row = lax.axis_index("kv") * own_rows
    arrived_max, arrived_totals, arrived_sums = (
        lax.all_to_all(
            leading(cache_part[0], token_count), "kv", split_axis=1, concat_axis=0, tiled=True
        ),
        lax.all_to_all(
            leading(cache_part[1], token_count), "kv", split_axis=1, concat_axis=0, tiled=True
        ),
        lax.all_to_all(
            leading(cache_part[2], token_count), "kv", split_axis=1, concat_axis=0, tiled=True
        ),
    )
    highest = jnp.max(arrived_max, axis=0)
    factors = jnp.exp(arrived_max - highest[None])
    folded = (
        highest,
        jnp.sum(arrived_totals * factors, axis=0),
        jnp.sum(arrived_sums * factors[..., None], axis=0),
    )
    own_tree = tuple(
        (
            lax.dynamic_slice_in_dim(
                member.reshape((token_count,) + member.shape[2:]), first_row, own_rows, 0
            )
            for member in tree_part
        )
    )
    finished = finish(combine(folded, own_tree), lambdas, head_gain).reshape(
        own_rows, local_heads * KDIM
    )
    normed = lax.all_gather(finished, "kv", axis=0, tiled=True)
    layer_out = lax.psum_scatter(
        jnp.dot(normed, w_out, preferred_element_type=jnp.float32).astype(jnp.bfloat16),
        "tp",
        scatter_dimension=0,
        tiled=True,
    )
    slot_of = positions[None, :, None] - limits[:, None, None]
    placing = (slot_of == jnp.arange(PROP, dtype=jnp.int32)[None, None, :]).astype(jnp.bfloat16)
    written = (jnp.sum(placing.astype(jnp.float32), axis=2) > 0.5)[:, :, None, None]
    placed_keys = jnp.einsum(
        "bpj,bjhd->bphd", placing, keys_fresh, preferred_element_type=jnp.float32
    ).astype(jnp.bfloat16)
    placed_values = jnp.einsum(
        "bpj,bjhd->bphd", placing, values_fresh, preferred_element_type=jnp.float32
    ).astype(jnp.bfloat16)
    keys_out = jnp.where(written, placed_keys, cache_keys)
    values_out = jnp.where(written, placed_values, cache_values)
    return (layer_out, keys_out, values_out)


def solution(mesh):
    return jax.shard_map(
        body,
        mesh=mesh,
        in_specs=(
            P(None, "kv"),
            P("kv"),
            P("kv", "tp"),
            P("kv", "tp"),
            P("kv", "tp"),
            P("tp"),
            P(),
            P("tp", "kv"),
            P(None, "kv", "tp", None),
            P(None, "kv", "tp", None),
            P(),
            P(),
            P(),
        ),
        out_specs=(P("tp", "kv"), P(None, "kv", "tp", None), P(None, "kv", "tp", None)),
        check_vma=False,
    )
```

profile of v0, /device:TPU:0, one launch (start us, length us, event | category | flops | bytes accessed | tf_op | source)
XLA Modules:
  0.0 199.4 jit_solution(11030734350312015369)
XLA Ops:
  7.2 1.1 copy-done
  8.4 1.9 fusion.40
  10.2 2.1 %fusion.42 = f32[128,512]{1,0:T(8,128)} fusion(bf16[512,512]{1,0:T(8,128)(2,1)} %param.16, bf16[128,512]{1,0:T(8,128)(2,1)} %param.13, f32[512]{0:T(512)} %param.14), kind=kOutput, calls=%fused_computation.56 | convolution fusion | flops 67305472 | bytes 919552 | tf_op jit(solution)/shard_map/dot_general | solution.py:87
  12.3 1.9 fusion.44
  14.3 23.6 %psum.28 = f32[128,1]{0,1:T(1,128)S(1)} all-reduce(f32[128,1]{0,1:T(1,128)S(1)} %bitcast.101), channel_id=1, replica_groups=mesh['kv'=8,'tp'=4] {'kv'}, use_global_device_ids=true, to_apply=%region_1.0 | all-reduce | flops 128 | bytes 1024 | tf_op jit(solution)/shard_map/psum | solution.py:89
  38.0 7.5 %copy.156 = bf16[8,512,4,128]{1,3,2,0:T(8,128)(2,1)} copy(bf16[8,512,4,128]{3,2,1,0:T(4,128)(2,1)} %param.21) | data formatting | bytes 8388608 | tf_op args[8]
  45.5 0.3 convolution_minimum_fusion.3
  45.7 0.2 convolution_minimum_fusion.2
  46.1 0.2 fusion.11
  46.6 0.7 broadcast_bitcast_fusion
  47.4 0.6 broadcast_compare_fusion
  48.0 44.8 %all-reduce.3.cloned.1.call-done = (f32[128,512]{1,0:T(8,128)}, f32[128,512]{1,0:T(8,128)}, f32[128,512]{1,0:T(8,128)}) async-done(((f32[128,512]{1,0:T(8,128)}, f32[128,512]{1,0:T(8,128)}, f32[128,512]{1,0:T(8,128)}), (f32[128,512]{1,0:T(8,128)}, f32[128,512]{1,0:T(8,128)}, f32[128,512]{1,0:T(8,128)})) %all-reduce.3.cloned.1.call-update) | async-done | bytes 786448 | tf_op jit(solution)/shard_map/psum | solution.py:89
  92.8 1.2 multiply_convert_fusion
  94.2 3.0 %bitcast_reduce_fusion = (f32[8,16,4,2]{1,3,2,0:T(2,128)S(1)}, f32[8,4,2,16,512]{4,3,2,1,0:T(8,128)S(1)}) fusion(pred[8,512]{1,0:T(8,128)(4,1)S(1)} %broadcast_compare_fusion.1, bf16[8,512,4,2,64]{1,4,3,2,0:T(8,128)(2,1)} %bitcast.84, bf16[8,16,4,2,64]{4,3,2,1,0:T(2,128)(2,1)S(1)} %reshape.160), kind=kOutput, calls=%fused_computation.5 | convolution fusion | flops 68680704 | bytes 6430720 | tf_op jit(solution)/shard_map/bjhmd,bphmd->bjhmp/dot_general | solution.py:109
  97.2 0.7 fusion.4
  98.2 0.8 reshape.183
  99.0 3.9 %all-to-all-start.2 = ((f32[8,1,128]{2,1,0:T(1,128)}), f32[8,1,128]{2,1,0:T(1,128)}, u32[]{:S(2)}, u32[]{:S(2)}) async-start(f32[8,1,128]{2,1,0:T(1,128)} %reshape.183), calls=%async_computation.2 | async-start | bytes 8192 | tf_op jit(solution)/shard_map/all_to_all | solution.py:127
  102.9 0.2 reshape.164
  103.1 4.0 %fusion.6 = f32[8,16,4,2,128]{4,1,3,2,0:T(8,128)} fusion(bf16[8,512,4,128,1]{3,2,1,0,4:T(4,128)(2,1)} %bitcast.102, f32[8,4,2,16,512]{4,3,2,1,0:T(8,128)S(1)} %get-tuple-element.41, f32[8,16,4,2]{1,3,2,0:T(2,128)S(1)} %get-tuple-element.40, pred[8,512]{1,0:T(8,128)(4,1)S(1)} %broadcast_compare_fusion.1), kind=kOutput, calls=%fused_computation.12 | convolution fusion | flops 136839168 | bytes 6823936 | tf_op jit(solution)/shard_map/bjhmp,bphd->bjhmd/dot_general | solution.py:44
  107.2 0.3 fusion.64
  107.5 0.3 convolution_bitcast_fusion
  108.0 0.8 reshape.181
  108.8 0.5 all-to-all-done.2
  109.3 5.4 %all-to-all-start.1 = ((f32[8,1,128]{2,1,0:T(1,128)}), f32[8,1,128]{2,1,0:T(1,128)S(1)}, u32[]{:S(2)}, u32[]{:S(2)}) async-start(f32[8,1,128]{2,1,0:T(1,128)} %reshape.181), calls=%async_computation.1 | async-start | bytes 8192 | tf_op jit(solution)/shard_map/all_to_all | solution.py:124
  114.7 0.2 fusion.19
  114.9 1.0 copy.200
  115.9 0.3 copy.205
  116.3 1.2 copy.160
  117.5 3.6 %all-to-all-done.1 = f32[8,1,128]{2,1,0:T(1,128)S(1)} async-done(((f32[8,1,128]{2,1,0:T(1,128)}), f32[8,1,128]{2,1,0:T(1,128)S(1)}, u32[]{:S(2)}, u32[]{:S(2)}) %all-to-all-start.1) | async-done | bytes 4128 | tf_op jit(solution)/shard_map/all_to_all | solution.py:124
  121.2 3.5 %all-to-all-start = ((f32[1,128,4,2,128]{4,3,2,0,1:T(2,128)}), f32[1,128,4,2,128]{4,3,2,0,1:T(2,128)S(1)}, u32[]{:S(2)}, u32[]{:S(2)}) async-start(f32[1,128,4,2,128]{4,3,2,0,1:T(2,128)} %copy.160), calls=%async_computation | async-start | bytes 1048576 | tf_op jit(solution)/shard_map/all_to_all | solution.py:130
  124.7 0.2 reduce-scatter.2.cloned.1.call-start
  124.9 3.6 %copy_select_fusion.1 = bf16[8,512,4,128]{3,1,2,0:T(8,128)(2,1)S(1)} fusion(bf16[8,512,4,128]{3,2,1,0:T(4,128)(2,1)} %param.21, pred[8,512]{1,0:T(8,128)(4,1)S(1)} %copy-done.12, bf16[8,16,4,128]{3,2,1,0:T(4,128)(2,1)S(1)} %reshape.170, s32[8,512]{1,0:T(8,128)S(1)} %copy-done.8), kind=kOutput, calls=%fused_computation.3 | convolution fusion | flops 71368704 | bytes 8540160 | tf_op jit(solution)/shard_map/bpj,bjhd->bphd/dot_general | solution.py:162
  128.5 5.3 %copy.189 = bf16[8,512,4,128]{3,2,1,0:T(4,128)(2,1)} copy(bf16[8,512,4,128]{3,1,2,0:T(8,128)(2,1)S(1)} %copy_select_fusion.1) | data formatting | bytes 8388608
  133.8 0.5 broadcast.113
  134.3 0.7 reduce.5
  134.9 0.2 reshape.182
  135.5 0.2 copy.210
  135.7 1.3 reduce.4
  137.1 0.2 reshape.184
  137.6 0.3 copy.166
  137.9 0.8 multiply_add_fusion
  138.7 0.7 multiply_reduce_fusion
  139.5 0.3 fusion.47
  140.2 30.8 %all_gather.3 = bf16[128,512]{1,0:T(8,128)(2,1)S(1)} all-gather(bf16[16,512]{1,0:T(8,128)(2,1)S(1)} %fusion.53), channel_id=1, replica_groups=mesh['kv'=8,'tp'=4] {'kv'}, dimensions={0}, use_global_device_ids=true | all-gather | bytes 147456 | tf_op jit(solution)/shard_map/all_gather | solution.py:152
  171.0 0.9 convolution_convert_fusion
  171.9 3.5 %copy_select_fusion = bf16[8,512,4,128]{3,1,2,0:T(8,128)(2,1)S(1)} fusion(bf16[8,512,4,128]{3,2,1,0:T(4,128)(2,1)} %param.22, pred[8,512]{1,0:T(8,128)(4,1)S(1)} %copy-done.12, bf16[8,16,4,128]{3,2,1,0:T(4,128)(2,1)S(1)} %reshape.166, s32[8,512]{1,0:T(8,128)S(1)} %copy-done.8), kind=kOutput, calls=%fused_computation.2 | convolution fusion | flops 71368704 | bytes 8540160 | tf_op jit(solution)/shard_map/bpj,bjhd->bphd/dot_general | solution.py:165
  175.5 5.3 %copy.190 = bf16[8,512,4,128]{3,2,1,0:T(4,128)(2,1)} copy(bf16[8,512,4,128]{3,1,2,0:T(8,128)(2,1)S(1)} %copy_select_fusion) | data formatting | bytes 8388608
  180.7 11.8 %reduce-scatter.2.cloned.1.call-done = bf16[32,512]{1,0:T(8,128)(2,1)} async-done(((bf16[128,512]{1,0:T(8,128)(2,1)}), bf16[32,512]{1,0:T(8,128)(2,1)}) %reduce-scatter.2.cloned.1.call-update) | async-done | bytes 32784 | tf_op jit(solution)/shard_map/reduce_scatter | solution.py:153
  (68 shorter events, 2.6 us)
Async XLA Ops:
  7.2 1.2 copy-start
  7.2 7.0 %copy-start.1 = (bf16[128,512]{1,0:T(8,128)(2,1)S(1)}, bf16[128,512]{1,0:T(8,128)(2,1)}, u32[]{:S(2)}) copy-start(bf16[128,512]{1,0:T(8,128)(2,1)} %param.13) | copy-start | bytes 393220
  7.2 5.1 %copy-start.2 = (bf16[512,512]{1,0:T(8,128)(2,1)S(1)}, bf16[512,512]{1,0:T(8,128)(2,1)}, u32[]{:S(2)}) copy-start(bf16[512,512]{1,0:T(8,128)(2,1)} %param.15) | copy-start | bytes 1572868
  7.2 85.6 %all-reduce.3.cloned.1.call-start = ((), (), s32[]{:S(2)}) async-start(), calls=%async_computation.5 | async-start | bytes 1572864 | tf_op jit(solution)/shard_map/psum | solution.py:89
  38.0 7.5 %copy-start.11 = (s32[8,16]{1,0:T(8,128)S(1)}, s32[8,16]{1,0:T(8,128)}, u32[]{:S(2)}) copy-start(s32[8,16]{1,0:T(8,128)} %param.25) | copy-start | bytes 1540
  38.0 8.5 %copy-start.16 = (s32[8]{0:T(128)S(1)}, s32[8]{0:T(128)}, u32[]{:S(2)}) copy-start(s32[8]{0:T(128)} %param.23) | copy-start | bytes 100
  38.0 8.5 %copy-start.17 = (s32[8]{0:T(128)S(1)}, s32[8]{0:T(128)}, u32[]{:S(2)}) copy-start(s32[8]{0:T(128)} %param.24) | copy-start | bytes 100
  38.0 8.6 %copy-start.13 = (f32[4]{0:T(128)S(1)}, f32[4]{0:T(128)}, u32[]{:S(2)}) copy-start(f32[4]{0:T(128)} %param.18) | copy-start | bytes 52
  38.0 8.6 %copy-start.15 = (f32[128]{0:T(128)S(1)}, f32[128]{0:T(128)}, u32[]{:S(2)}) copy-start(f32[128]{0:T(128)} %param.19) | copy-start | bytes 1540
  46.5 47.7 %copy-start.7 = (s32[8,512]{1,0:T(8,128)}, s32[8,512]{1,0:T(8,128)S(1)}, u32[]{:S(2)}) copy-start(s32[8,512]{1,0:T(8,128)S(1)} %broadcast_subtract_fusion) | copy-start | bytes 49156
  97.2 9.9 %copy-start.5 = (f32[8,16,4,2]{1,3,2,0:T(2,128)}, f32[8,16,4,2]{1,3,2,0:T(2,128)S(1)}, u32[]{:S(2)}) copy-start(f32[8,16,4,2]{1,3,2,0:T(2,128)S(1)} %get-tuple-element.40) | copy-start | bytes 12292
  99.0 10.3 %all-to-all-start.2 = ((f32[8,1,128]{2,1,0:T(1,128)}), f32[8,1,128]{2,1,0:T(1,128)}, u32[]{:S(2)}, u32[]{:S(2)}) async-start(f32[8,1,128]{2,1,0:T(1,128)} %reshape.183), calls=%async_computation.2 | async-start | bytes 8192 | tf_op jit(solution)/shard_map/all_to_all | solution.py:127
  107.1 0.8 copy-start.6
  107.1 9.1 %copy-start.4 = (f32[8,16,4,2,128]{4,1,3,2,0:T(8,128)S(1)}, f32[8,16,4,2,128]{4,1,3,2,0:T(8,128)}, u32[]{:S(2)}) copy-start(f32[8,16,4,2,128]{4,1,3,2,0:T(8,128)} %fusion.6) | copy-start | bytes 1572868
  109.3 11.9 %all-to-all-start.1 = ((f32[8,1,128]{2,1,0:T(1,128)}), f32[8,1,128]{2,1,0:T(1,128)S(1)}, u32[]{:S(2)}, u32[]{:S(2)}) async-start(f32[8,1,128]{2,1,0:T(1,128)} %reshape.181), calls=%async_computation.1 | async-start | bytes 8192 | tf_op jit(solution)/shard_map/all_to_all | solution.py:124
  116.2 8.7 %copy-start.8 = (s32[8,512]{1,0:T(8,128)S(1)}, s32[8,512]{1,0:T(8,128)}, u32[]{:S(2)}) copy-start(s32[8,512]{1,0:T(8,128)} %copy-done.7) | copy-start | bytes 49156
  116.2 8.7 %copy-start.12 = (pred[8,512]{1,0:T(8,128)(4,1)S(1)}, pred[8,512]{1,0:T(8,128)(4,1)}, u32[]{:S(2)}) copy-start(pred[8,512]{1,0:T(8,128)(4,1)} %broadcast_compare_fusion) | copy-start | bytes 12292
  121.2 17.6 %all-to-all-start = ((f32[1,128,4,2,128]{4,3,2,0,1:T(2,128)}), f32[1,128,4,2,128]{4,3,2,0,1:T(2,128)S(1)}, u32[]{:S(2)}, u32[]{:S(2)}) async-start(f32[1,128,4,2,128]{4,3,2,0,1:T(2,128)} %copy.160), calls=%async_computation | async-start | bytes 1048576 | tf_op jit(solution)/shard_map/all_to_all | solution.py:130
  124.7 67.9 %reduce-scatter.2.cloned.1.call-start = ((), (), s32[]{:S(2)}) async-start(), calls=%async_computation.4 | async-start | bytes 163840 | tf_op jit(solution)/shard_map/reduce_scatter | solution.py:153
  133.7 6.1 %copy-start.14 = (f32[4]{0:T(128)S(1)}, f32[4]{0:T(128)}, u32[]{:S(2)}) copy-start(f32[4]{0:T(128)} %param.18) | copy-start | bytes 52
  133.7 6.4 %copy-start.9 = (f32[512]{0:T(512)S(1)}, f32[512]{0:T(512)}, u32[]{:S(2)}) copy-start(f32[512]{0:T(512)} %get-tuple-element.42) | copy-start | bytes 6148
  133.7 6.4 %copy-start.10 = (f32[512]{0:T(512)S(1)}, f32[512]{0:T(512)}, u32[]{:S(2)}) copy-start(f32[512]{0:T(512)} %get-tuple-element.43) | copy-start | bytes 6148
  133.7 37.3 %copy-start.3 = (bf16[512,512]{1,0:T(8,128)(2,1)S(1)}, bf16[512,512]{1,0:T(8,128)(2,1)}, u32[]{:S(2)}) copy-start(bf16[512,512]{1,0:T(8,128)(2,1)} %param.20) | copy-start | bytes 1572868
Sparse Core Ops, SparseCore 0:
  14.3 78.4 all-reduce.2
  172.0 20.4 reduce-scatter.1
where the time goes:
time: 200 us; the launch traced here: 199 us
  waiting for transfers between devices  60.8 us (30%)
  blocking collectives  54.5 us (27%)
  local copies, waits for them, and re-layouts  27.1 us (14%)
  matrix products  22.2 us (11%)
  between operations  14.5 us (7%)
  starting transfers between devices  13.1 us (7%)
  other arithmetic  7.19 us (4%)
    psum x1, waiting for transfers between devices, body(): lax.psum((part_query, part_key, part_value, squares_local), 'kv')  44.8 us
    all_gather x1, blocking collectives, body(): normed = lax.all_gather(finished, 'kv', axis=0, tiled=True)  30.8 us
    psum x1, blocking collectives, body(): lax.psum((part_query, part_key, part_value, squares_local), 'kv')  23.6 us
    unnamed x45, local copies, waits for them, and re-layouts  21.6 us
    reduce_scatter x1, waiting for transfers between devices, body(): lax.psum_scatter(jnp.dot(normed, w_out, preferred_element_type=jnp.float3...  11.8 us
    all_to_all x1, starting transfers between devices, body(): lax.all_to_all(leading(cache_part[0], token_count), 'kv', split_axis=1, c...  5.43 us
    dot_general x2, matrix products, softmax_block(): jnp.einsum('bjhmp,bphd->bjhmd', weights.astype(jnp.bfloat16), values, pre...  4.32 us
  transfers between devices with their start and end apart: 5, of which 4 were waited for; matrix products, arithmetic and copies ran while one was open for 21% of the time, Pallas kernels for 0%

commit v1 on v0

--- a/solution.py
+++ b/solution.py
@@ -149,7 +149,12 @@
     finished = finish(combine(folded, own_tree), lambdas, head_gain).reshape(
         own_rows, local_heads * KDIM
     )
-    normed = lax.all_gather(finished, "kv", axis=0, tiled=True)
+    ring = [finished]
+    for hop in range(7):
+        ring.append(lax.ppermute(ring[-1], "kv", [(dev, (dev + 1) % 8) for dev in range(8)]))
+    normed = jnp.roll(
+        jnp.concatenate(ring[::-1], axis=0), (lax.axis_index("kv") + 1) * ring[0].shape[0], axis=0
+    )
     layer_out = lax.psum_scatter(
         jnp.dot(normed, w_out, preferred_element_type=jnp.float32).astype(jnp.bfloat16),
         "tp",

time: 200 us -> 214 us (1.070)
  waiting for transfers between devices: 60.8 us -> 109 us
  blocking collectives: 54.5 us -> 23.3 us
    ppermute x0 -> x7, waiting for transfers between devices: none -> 36.9 us  [body(): lax.ppermute(ring[-1], 'kv', [(dev, (dev + 1) % 8) for dev in range(8)])]
    all_gather x1 -> x0, blocking collectives: 30.8 us -> none  [body(): normed = lax.all_gather(finished, 'kv', axis=0, tiled=True)]
    all_to_all x1, waiting for transfers between devices: 0.01 us -> 7.21 us  [body(): lax.all_to_all(leading(cache_part[2], token_count), 'kv', split_axis=1, c...]
    unnamed x45 -> x44, local copies, waits for them, and re-layouts: 21.6 us -> 21.5 us
  transfers between devices with their start and end apart: 5 -> 12, of which waited for: 4 -> 11; matrix products, arithmetic and copies ran while one was open for 21% -> 18% of each run, Pallas kernels for 0% -> 0%
where the time goes in v1:
time: 214 us
  waiting for transfers between devices  109 us (51%)
  local copies, waits for them, and re-layouts  25.8 us (12%)
  blocking collectives  23.3 us (11%)
  matrix products  22.3 us (10%)
  between operations  14.6 us (7%)
  starting transfers between devices  13.8 us (6%)
  other arithmetic  5.18 us (2%)
    psum x1, waiting for transfers between devices, body(): lax.psum((part_query, part_key, part_value, squares_local), 'kv')  46.5 us
    ppermute x7, waiting for transfers between devices, body(): lax.ppermute(ring[-1], 'kv', [(dev, (dev + 1) % 8) for dev in range(8)])  36.9 us
    psum x1, blocking collectives, body(): lax.psum((part_query, part_key, part_value, squares_local), 'kv')  23.3 us
    unnamed x44, local copies, waits for them, and re-layouts  21.5 us
    reduce_scatter x1, waiting for transfers between devices, body(): lax.psum_scatter(jnp.dot(normed, w_out, preferred_element_type=jnp.float3...  12.4 us
    all_to_all x1, waiting for transfers between devices, body(): lax.all_to_all(leading(cache_part[2], token_count), 'kv', split_axis=1, c...  7.21 us
    all_to_all x1, starting transfers between devices, body(): lax.all_to_all(leading(cache_part[0], token_count), 'kv', split_axis=1, c...  4.87 us
    all_to_all x1, waiting for transfers between devices, body(): lax.all_to_all(leading(cache_part[0], token_count), 'kv', split_axis=1, c...  4.57 us
  transfers between devices with their start and end apart: 12, of which 11 were waited for; matrix products, arithmetic and copies ran while one was open for 18% of the time, Pallas kernels for 0%

profile of v1, /device:TPU:0, one launch (start us, length us, event | category | flops | bytes accessed | tf_op | source)
XLA Modules:
  0.0 213.6 jit_solution(17452914201273674330)
XLA Ops:
  7.3 1.1 copy-done
  8.4 1.9 fusion.41
  10.2 2.1 fusion.43
  12.3 1.9 fusion.45
  14.2 0.3 convolution_minimum_fusion.3
  15.3 7.4 %copy.156 = bf16[8,512,4,128]{1,3,2,0:T(8,128)(2,1)} copy(bf16[8,512,4,128]{3,2,1,0:T(4,128)(2,1)} %param.21) | data formatting | bytes 8388608 | tf_op args[8]
  22.8 23.3 %psum.28 = f32[128,1]{0,1:T(1,128)S(1)} all-reduce(f32[128,1]{0,1:T(1,128)S(1)} %bitcast.100), channel_id=1, replica_groups=mesh['kv'=8,'tp'=4] {'kv'}, use_global_device_ids=true, to_apply=%region_1.0 | all-reduce | flops 128 | bytes 1024 | tf_op jit(solution)/shard_map/psum | solution.py:89
  46.3 46.5 %all-reduce.3.cloned.1.call-done = (f32[128,512]{1,0:T(8,128)}, f32[128,512]{1,0:T(8,128)}, f32[128,512]{1,0:T(8,128)}) async-done(((f32[128,512]{1,0:T(8,128)}, f32[128,512]{1,0:T(8,128)}, f32[128,512]{1,0:T(8,128)}), (f32[128,512]{1,0:T(8,128)}, f32[128,512]{1,0:T(8,128)}, f32[128,512]{1,0:T(8,128)})) %all-reduce.3.cloned.1.call-update) | async-done | bytes 786448 | tf_op jit(solution)/shard_map/psum | solution.py:89
  92.8 1.2 multiply_convert_fusion
  94.2 3.0 %bitcast_reduce_fusion = (f32[8,16,4,2]{1,3,2,0:T(2,128)S(1)}, f32[8,4,2,16,512]{4,3,2,1,0:T(8,128)S(1)}) fusion(pred[8,512]{1,0:T(8,128)(4,1)S(1)} %broadcast_compare_fusion.1, bf16[8,512,4,2,64]{1,4,3,2,0:T(8,128)(2,1)} %bitcast.83, bf16[8,16,4,2,64]{4,3,2,1,0:T(2,128)(2,1)S(1)} %reshape.160), kind=kOutput, calls=%fused_computation.5 | convolution fusion | flops 68680704 | bytes 6430720 | tf_op jit(solution)/shard_map/bjhmd,bphmd->bjhmp/dot_general | solution.py:109
  97.2 0.8 fusion.4
  98.2 0.8 reshape.183
  99.0 3.8 %all-to-all-start.2 = ((f32[8,1,128]{2,1,0:T(1,128)}), f32[8,1,128]{2,1,0:T(1,128)S(1)}, u32[]{:S(2)}, u32[]{:S(2)}) async-start(f32[8,1,128]{2,1,0:T(1,128)} %reshape.183), calls=%async_computation.2 | async-start | bytes 8192 | tf_op jit(solution)/shard_map/all_to_all | solution.py:127
  102.7 4.1 %fusion.6 = f32[8,16,4,2,128]{4,1,3,2,0:T(8,128)} fusion(bf16[8,512,4,128,1]{3,2,1,0,4:T(4,128)(2,1)} %bitcast.101, f32[8,4,2,16,512]{4,3,2,1,0:T(8,128)S(1)} %get-tuple-element.41, f32[8,16,4,2]{1,3,2,0:T(2,128)S(1)} %get-tuple-element.40, pred[8,512]{1,0:T(8,128)(4,1)S(1)} %broadcast_compare_fusion.1), kind=kOutput, calls=%fused_computation.12 | convolution fusion | flops 136839168 | bytes 6823936 | tf_op jit(solution)/shard_map/bjhmp,bphd->bjhmd/dot_general | solution.py:44
  107.0 0.8 reshape.181
  108.0 1.2 all-to-all-done.2
  109.1 4.9 %all-to-all-start.1 = ((f32[8,1,128]{2,1,0:T(1,128)}), f32[8,1,128]{2,1,0:T(1,128)S(1)}, u32[]{:S(2)}, u32[]{:S(2)}) async-start(f32[8,1,128]{2,1,0:T(1,128)} %reshape.181), calls=%async_computation.1 | async-start | bytes 8192 | tf_op jit(solution)/shard_map/all_to_all | solution.py:124
  114.0 0.3 fusion.66
  114.3 0.3 copy.200
  114.7 1.2 copy.160
  115.9 4.6 %all-to-all-done.1 = f32[8,1,128]{2,1,0:T(1,128)S(1)} async-done(((f32[8,1,128]{2,1,0:T(1,128)}), f32[8,1,128]{2,1,0:T(1,128)S(1)}, u32[]{:S(2)}, u32[]{:S(2)}) %all-to-all-start.1) | async-done | bytes 4128 | tf_op jit(solution)/shard_map/all_to_all | solution.py:124
  120.4 3.5 %all-to-all-start = ((f32[1,128,4,2,128]{4,3,2,0,1:T(2,128)}), f32[1,128,4,2,128]{4,3,2,0,1:T(2,128)S(1)}, u32[]{:S(2)}, u32[]{:S(2)}) async-start(f32[1,128,4,2,128]{4,3,2,0,1:T(2,128)} %copy.160), calls=%async_computation | async-start | bytes 1048576 | tf_op jit(solution)/shard_map/all_to_all | solution.py:130
  124.0 0.2 fusion.19
  124.2 0.3 copy.205
  124.5 0.3 convolution_bitcast_fusion
  124.9 0.5 broadcast.114
  125.4 0.7 reduce.5
  126.0 0.2 reshape.182
  126.6 0.2 copy.210
  126.8 0.7 reduce.4
  127.5 0.2 reshape.184
  128.1 0.3 copy.166
  128.4 7.2 %all-to-all-done = f32[1,128,4,2,128]{4,3,2,0,1:T(2,128)S(1)} async-done(((f32[1,128,4,2,128]{4,3,2,0,1:T(2,128)}), f32[1,128,4,2,128]{4,3,2,0,1:T(2,128)S(1)}, u32[]{:S(2)}, u32[]{:S(2)}) %all-to-all-start) | async-done | bytes 524320 | tf_op jit(solution)/shard_map/all_to_all | solution.py:130
  135.6 0.7 multiply_reduce_fusion
  136.3 0.3 fusion.48
  137.0 1.6 collective-permute-start
  138.6 4.9 %collective-permute-done = bf16[16,512]{1,0:T(8,128)(2,1)S(1)} collective-permute-done((bf16[16,512]{1,0:T(8,128)(2,1)S(1)}, bf16[16,512]{1,0:T(8,128)(2,1)S(1)}, u32[]{:S(2)}, u32[]{:S(2)}) %collective-permute-start) | collective-permute-done | bytes 16416 | tf_op jit(solution)/shard_map/ppermute | solution.py:154
  143.5 6.4 %collective-permute-done.1 = bf16[16,512]{1,0:T(8,128)(2,1)S(1)} collective-permute-done((bf16[16,512]{1,0:T(8,128)(2,1)S(1)}, bf16[16,512]{1,0:T(8,128)(2,1)S(1)}, u32[]{:S(2)}, u32[]{:S(2)}) %collective-permute-start.1) | collective-permute-done | bytes 16416 | tf_op jit(solution)/shard_map/ppermute | solution.py:154
  150.0 6.4 %collective-permute-done.2 = bf16[16,512]{1,0:T(8,128)(2,1)S(1)} collective-permute-done((bf16[16,512]{1,0:T(8,128)(2,1)S(1)}, bf16[16,512]{1,0:T(8,128)(2,1)S(1)}, u32[]{:S(2)}, u32[]{:S(2)}) %collective-permute-start.2) | collective-permute-done | bytes 16416 | tf_op jit(solution)/shard_map/ppermute | solution.py:154
  156.5 6.4 %collective-permute-done.3 = bf16[16,512]{1,0:T(8,128)(2,1)S(1)} collective-permute-done((bf16[16,512]{1,0:T(8,128)(2,1)S(1)}, bf16[16,512]{1,0:T(8,128)(2,1)S(1)}, u32[]{:S(2)}, u32[]{:S(2)}) %collective-permute-start.3) | collective-permute-done | bytes 16416 | tf_op jit(solution)/shard_map/ppermute | solution.py:154
  162.9 6.4 %collective-permute-done.4 = bf16[16,512]{1,0:T(8,128)(2,1)S(1)} collective-permute-done((bf16[16,512]{1,0:T(8,128)(2,1)S(1)}, bf16[16,512]{1,0:T(8,128)(2,1)S(1)}, u32[]{:S(2)}, u32[]{:S(2)}) %collective-permute-start.4) | collective-permute-done | bytes 16416 | tf_op jit(solution)/shard_map/ppermute | solution.py:154
  169.3 6.4 %collective-permute-done.5 = bf16[16,512]{1,0:T(8,128)(2,1)S(1)} collective-permute-done((bf16[16,512]{1,0:T(8,128)(2,1)S(1)}, bf16[16,512]{1,0:T(8,128)(2,1)S(1)}, u32[]{:S(2)}, u32[]{:S(2)}) %collective-permute-start.5) | collective-permute-done | bytes 16416 | tf_op jit(solution)/shard_map/ppermute | solution.py:154
  175.7 3.5 %copy_select_fusion.1 = bf16[8,512,4,128]{3,1,2,0:T(8,128)(2,1)S(1)} fusion(bf16[8,512,4,128]{3,2,1,0:T(4,128)(2,1)} %param.21, pred[8,512]{1,0:T(8,128)(4,1)S(1)} %broadcast_compare_fusion, bf16[8,16,4,128]{3,2,1,0:T(4,128)(2,1)S(1)} %reshape.170, s32[8,512]{1,0:T(8,128)S(1)} %broadcast_subtract_fusion), kind=kOutput, calls=%fused_computation.3 | convolution fusion | flops 71368704 | bytes 8540160 | tf_op jit(solution)/shard_map/bpj,bjhd->bphd/dot_general | solution.py:167
  179.3 5.3 %copy.189 = bf16[8,512,4,128]{3,2,1,0:T(4,128)(2,1)} copy(bf16[8,512,4,128]{3,1,2,0:T(8,128)(2,1)S(1)} %copy_select_fusion.1) | data formatting | bytes 8388608
  184.7 0.9 convolution_convert_fusion
  185.6 3.6 %copy_select_fusion = bf16[8,512,4,128]{3,1,2,0:T(8,128)(2,1)S(1)} fusion(bf16[8,512,4,128]{3,2,1,0:T(4,128)(2,1)} %param.22, pred[8,512]{1,0:T(8,128)(4,1)S(1)} %broadcast_compare_fusion, bf16[8,16,4,128]{3,2,1,0:T(4,128)(2,1)S(1)} %reshape.166, s32[8,512]{1,0:T(8,128)S(1)} %broadcast_subtract_fusion), kind=kOutput, calls=%fused_computation.2 | convolution fusion | flops 71368704 | bytes 8540160 | tf_op jit(solution)/shard_map/bpj,bjhd->bphd/dot_general | solution.py:170
  189.2 5.3 %copy.190 = bf16[8,512,4,128]{3,2,1,0:T(4,128)(2,1)} copy(bf16[8,512,4,128]{3,1,2,0:T(8,128)(2,1)S(1)} %copy_select_fusion) | data formatting | bytes 8388608
  194.4 12.4 %reduce-scatter.2.cloned.1.call-done = bf16[32,512]{1,0:T(8,128)(2,1)} async-done(((bf16[128,512]{1,0:T(8,128)(2,1)}), bf16[32,512]{1,0:T(8,128)(2,1)}) %reduce-scatter.2.cloned.1.call-update) | async-done | bytes 32784 | tf_op jit(solution)/shard_map/reduce_scatter | solution.py:158
  (81 shorter events, 3.3 us)
Async XLA Ops:
  7.2 1.2 copy-start
  7.2 7.9 %copy-start.1 = (bf16[128,512]{1,0:T(8,128)(2,1)S(1)}, bf16[128,512]{1,0:T(8,128)(2,1)}, u32[]{:S(2)}) copy-start(bf16[128,512]{1,0:T(8,128)(2,1)} %param.13) | copy-start | bytes 393220
  7.2 5.1 %copy-start.2 = (bf16[512,512]{1,0:T(8,128)(2,1)S(1)}, bf16[512,512]{1,0:T(8,128)(2,1)}, u32[]{:S(2)}) copy-start(bf16[512,512]{1,0:T(8,128)(2,1)} %param.15) | copy-start | bytes 1572868
  7.2 7.0 %copy-start.5 = (s32[8,16]{1,0:T(8,128)S(1)}, s32[8,16]{1,0:T(8,128)}, u32[]{:S(2)}) copy-start(s32[8,16]{1,0:T(8,128)} %param.25) | copy-start | bytes 1540
  7.2 85.6 %all-reduce.3.cloned.1.call-start = ((), (), s32[]{:S(2)}) async-start(), calls=%async_computation.5 | async-start | bytes 1572864 | tf_op jit(solution)/shard_map/psum | solution.py:89
  15.2 7.6 %copy-start.8 = (s32[8]{0:T(128)S(1)}, s32[8]{0:T(128)}, u32[]{:S(2)}) copy-start(s32[8]{0:T(128)} %param.23) | copy-start | bytes 100
  15.2 7.6 %copy-start.9 = (s32[8]{0:T(128)S(1)}, s32[8]{0:T(128)}, u32[]{:S(2)}) copy-start(s32[8]{0:T(128)} %param.24) | copy-start | bytes 100
  15.2 30.9 %copy-start.6 = (f32[4]{0:T(128)S(1)}, f32[4]{0:T(128)}, u32[]{:S(2)}) copy-start(f32[4]{0:T(128)} %param.18) | copy-start | bytes 52
  15.2 30.9 %copy-start.7 = (f32[128]{0:T(128)S(1)}, f32[128]{0:T(128)}, u32[]{:S(2)}) copy-start(f32[128]{0:T(128)} %param.19) | copy-start | bytes 1540
  99.0 10.2 %all-to-all-start.2 = ((f32[8,1,128]{2,1,0:T(1,128)}), f32[8,1,128]{2,1,0:T(1,128)S(1)}, u32[]{:S(2)}, u32[]{:S(2)}) async-start(f32[8,1,128]{2,1,0:T(1,128)} %reshape.183), calls=%async_computation.2 | async-start | bytes 8192 | tf_op jit(solution)/shard_map/all_to_all | solution.py:127
  106.8 7.8 %copy-start.4 = (f32[8,16,4,2,128]{4,1,3,2,0:T(8,128)S(1)}, f32[8,16,4,2,128]{4,1,3,2,0:T(8,128)}, u32[]{:S(2)}) copy-start(f32[8,16,4,2,128]{4,1,3,2,0:T(8,128)} %fusion.6) | copy-start | bytes 1572868
  109.1 11.3 %all-to-all-start.1 = ((f32[8,1,128]{2,1,0:T(1,128)}), f32[8,1,128]{2,1,0:T(1,128)S(1)}, u32[]{:S(2)}, u32[]{:S(2)}) async-start(f32[8,1,128]{2,1,0:T(1,128)} %reshape.181), calls=%async_computation.1 | async-start | bytes 8192 | tf_op jit(solution)/shard_map/all_to_all | solution.py:124
  120.4 15.2 %all-to-all-start = ((f32[1,128,4,2,128]{4,3,2,0,1:T(2,128)}), f32[1,128,4,2,128]{4,3,2,0,1:T(2,128)S(1)}, u32[]{:S(2)}, u32[]{:S(2)}) async-start(f32[1,128,4,2,128]{4,3,2,0,1:T(2,128)} %copy.160), calls=%async_computation | async-start | bytes 1048576 | tf_op jit(solution)/shard_map/all_to_all | solution.py:130
  123.9 82.9 %reduce-scatter.2.cloned.1.call-start = ((), (), s32[]{:S(2)}) async-start(), calls=%async_computation.4 | async-start | bytes 163840 | tf_op jit(solution)/shard_map/reduce_scatter | solution.py:158
  137.0 6.5 %collective-permute-start = (bf16[16,512]{1,0:T(8,128)(2,1)S(1)}, bf16[16,512]{1,0:T(8,128)(2,1)S(1)}, u32[]{:S(2)}, u32[]{:S(2)}) collective-permute-start(bf16[16,512]{1,0:T(8,128)(2,1)S(1)} %fusion.54), channel_id=1, source_target_pairs={{0,4},{4,8},{8,12},{12,16},{16,20},{20,24},{24,28},{28,0},{1,5},{5... | collective-permute-start | bytes 49160 | tf_op jit(solution)/shard_map/ppermute | solution.py:154
  143.5 6.4 %collective-permute-start.1 = (bf16[16,512]{1,0:T(8,128)(2,1)S(1)}, bf16[16,512]{1,0:T(8,128)(2,1)S(1)}, u32[]{:S(2)}, u32[]{:S(2)}) collective-permute-start(bf16[16,512]{1,0:T(8,128)(2,1)S(1)} %collective-permute-done), channel_id=1, source_target_pairs={{0,4},{4,8},{8,12},{12,16},{16,20},{20,24},{24,28},{28,0},{1,5},{5... | collective-permute-start | bytes 49160 | tf_op jit(solution)/shard_map/ppermute | solution.py:154
  150.0 6.4 %collective-permute-start.2 = (bf16[16,512]{1,0:T(8,128)(2,1)S(1)}, bf16[16,512]{1,0:T(8,128)(2,1)S(1)}, u32[]{:S(2)}, u32[]{:S(2)}) collective-permute-start(bf16[16,512]{1,0:T(8,128)(2,1)S(1)} %collective-permute-done.1), channel_id=1, source_target_pairs={{0,4},{4,8},{8,12},{12,16},{16,20},{20,24},{24,28},{28,0},{1,5},{5... | collective-permute-start | bytes 49160 | tf_op jit(solution)/shard_map/ppermute | solution.py:154
  156.4 6.4 %collective-permute-start.3 = (bf16[16,512]{1,0:T(8,128)(2,1)S(1)}, bf16[16,512]{1,0:T(8,128)(2,1)S(1)}, u32[]{:S(2)}, u32[]{:S(2)}) collective-permute-start(bf16[16,512]{1,0:T(8,128)(2,1)S(1)} %collective-permute-done.2), channel_id=1, source_target_pairs={{0,4},{4,8},{8,12},{12,16},{16,20},{20,24},{24,28},{28,0},{1,5},{5... | collective-permute-start | bytes 49160 | tf_op jit(solution)/shard_map/ppermute | solution.py:154
  162.8 6.4 %collective-permute-start.4 = (bf16[16,512]{1,0:T(8,128)(2,1)S(1)}, bf16[16,512]{1,0:T(8,128)(2,1)S(1)}, u32[]{:S(2)}, u32[]{:S(2)}) collective-permute-start(bf16[16,512]{1,0:T(8,128)(2,1)S(1)} %collective-permute-done.3), channel_id=1, source_target_pairs={{0,4},{4,8},{8,12},{12,16},{16,20},{20,24},{24,28},{28,0},{1,5},{5... | collective-permute-start | bytes 49160 | tf_op jit(solution)/shard_map/ppermute | solution.py:154
  169.3 6.4 %collective-permute-start.5 = (bf16[16,512]{1,0:T(8,128)(2,1)S(1)}, bf16[16,512]{1,0:T(8,128)(2,1)S(1)}, u32[]{:S(2)}, u32[]{:S(2)}) collective-permute-start(bf16[16,512]{1,0:T(8,128)(2,1)S(1)} %collective-permute-done.4), channel_id=1, source_target_pairs={{0,4},{4,8},{8,12},{12,16},{16,20},{20,24},{24,28},{28,0},{1,5},{5... | collective-permute-start | bytes 49160 | tf_op jit(solution)/shard_map/ppermute | solution.py:154
  175.7 8.8 %collective-permute-start.6 = (bf16[16,512]{1,0:T(8,128)(2,1)S(1)}, bf16[16,512]{1,0:T(8,128)(2,1)S(1)}, u32[]{:S(2)}, u32[]{:S(2)}) collective-permute-start(bf16[16,512]{1,0:T(8,128)(2,1)S(1)} %collective-permute-done.5), channel_id=1, source_target_pairs={{0,4},{4,8},{8,12},{12,16},{16,20},{20,24},{24,28},{28,0},{1,5},{5... | collective-permute-start | bytes 49160 | tf_op jit(solution)/shard_map/ppermute | solution.py:154
  179.3 5.4 %copy-start.3 = (bf16[512,512]{1,0:T(8,128)(2,1)S(1)}, bf16[512,512]{1,0:T(8,128)(2,1)}, u32[]{:S(2)}) copy-start(bf16[512,512]{1,0:T(8,128)(2,1)} %param.20) | copy-start | bytes 1572868
Sparse Core Ops, SparseCore 0:
  14.3 78.4 all-reduce.2
  185.7 21.0 reduce-scatter.1
